TPU v7x, 32 devices: a whole 2x2x4 slice. The times are simulated.
32 devices in a mesh: dp: 4 (over y, x), kv: 4 (over z), tp: 2 (over core).
Axes of the slice: x: 2, y: 2, z: 4, core: 2. Of those that a mesh axis runs over, the one named last changes fastest.
Arguments:
- tokens: bfloat16 [128, 4096], P('dp', ('kv', 'tp')), parts along dimension 0, may hold values from -12 to 12
- norm_gain: float32 [4096], replicated, may hold values from 0.1 to 1.9
- w_query: bfloat16 [4096, 3072], P(None, ('kv', 'tp')), may hold values from -0.09375 to 0.09375
- w_key: bfloat16 [4096, 3072], P(None, ('kv', 'tp')), may hold values from -0.09375 to 0.09375
- w_value: bfloat16 [4096, 3072], P(None, ('kv', 'tp')), may hold values from -0.09375 to 0.09375
- w_gate: bfloat16 [4096, 3072], P(None, ('kv', 'tp')), may hold values from -0.09375 to 0.09375
- w_output: bfloat16 [3072, 4096], P(None, ('kv', 'tp')), may hold values from -0.109375 to 0.109375
- decay_rate: float32 [24], replicated, may hold values from 0.003 to 2
- state: float32 [32, 24, 128, 128], P(('dp', 'kv', 'tp')), parts along dimension 0, may hold values from -0.54 to 0.54
- prev_keys: bfloat16 [32, 4, 3072], P(('dp', 'kv', 'tp')), parts along dimension 0, may hold values from -0.5390625 to 0.5390625
- prev_values: bfloat16 [32, 4, 3072], P(('dp', 'kv', 'tp')), parts along dimension 0, may hold values from -6 to 6
- accepted: int32 [32], P(('dp', 'kv', 'tp')), parts along dimension 0, may hold values from 0 to 4
- parents: int32 [32, 4], P(('dp', 'kv', 'tp')), parts along dimension 0, may hold values from -1 to 2, as said below
- seq_length: int32 [32], P(('dp', 'kv', 'tp')), parts along dimension 0, may hold values from 1 to 8191
Outputs:
- output: bfloat16 [128, 4096], P('dp', ('kv', 'tp')), parts along dimension 0
- carried: float32 [32, 24, 128, 128], P(('dp', 'kv', 'tp')), parts along dimension 0
There are 4 independent parts, one for each index of `dp`. A program takes and returns all parts, laid end to end along the dimension named above; an argument that names none is the same for every part. Nothing has to cross between parts.
Inputs may be any that keep to these rules, and one draw needn't show every extreme that they name: parents[s, i] is -1 or an earlier proposal of the same sequence; proposal 0 has -1.
All inputs are finite; a program needn't handle non-finite values.
Results may differ from a plain program's by a relative error of at most 0.013.
Values may be sent and summed in bfloat16 or wider, within the bound.
A program may use at most 64 MiB of HBM per device.

v0:
```python
import jax
import jax.numpy as jnp
from jax import lax
from jax.sharding import PartitionSpec as P

EPS = 1e-06
HIGH = lax.Precision.HIGHEST


def rotate(tensor, positions):
    half_dim = tensor.shape[-1] // 2
    frequency = 10000.0 ** (-jnp.arange(half_dim, dtype=jnp.float32) / half_dim)
    angles = positions[:, :, None] * frequency[None, None, :]
    cosine = jnp.cos(angles)[:, :, None, :]
    sine_part = jnp.sin(angles)[:, :, None, :]
    first = tensor[..., :half_dim]
    second = tensor[..., half_dim:]
    return jnp.concatenate(
        [first * cosine - second * sine_part, second * cosine + first * sine_part], axis=-1
    )


def ancestry_of(parents):
    props = parents.shape[1]
    linked = (parents[:, :, None] == jnp.arange(props, dtype=jnp.int32)[None, None, :]).astype(
        jnp.float32
    )
    identity = jnp.broadcast_to(jnp.eye(props, dtype=jnp.float32), linked.shape)
    ancestry = identity
    power = identity
    for hop in range(props - 1):
        power = jnp.einsum("bij,bjk->bik", power, linked, precision=HIGH)
        ancestry = ancestry + power
    depths = jnp.sum(ancestry, axis=-1) - 1.0
    return (ancestry, depths)


def advance(state, prev_keys, prev_values, accepted, decays):
    nseq, props, width = prev_keys.shape
    heads = decays.shape[0]
    head_dim = width // heads
    old_keys = prev_keys.astype(jnp.float32).reshape(nseq, props, heads, head_dim)
    old_values = prev_values.astype(jnp.float32).reshape(nseq, props, heads, head_dim)
    steps_done = accepted.astype(jnp.float32)[:, None]
    index = jnp.arange(props, dtype=jnp.float32)[None, :]
    age = jnp.maximum(steps_done - 1.0 - index, 0.0)
    weights = jnp.where(
        (index < steps_done)[:, :, None], jnp.exp(-decays[None, None, :] * age[:, :, None]), 0.0
    )
    kept = jnp.exp(-decays[None, :] * steps_done)
    added = jnp.einsum("bphd,bphe->bhde", old_keys * weights[..., None], old_values, precision=HIGH)
    return kept[:, :, None, None] * state + added


def retain(queries, key_rows, val_rows, gate_rows, decays, carried, parents, accepted, seq_length):
    nseq, props, heads, head_dim = queries.shape
    ancestry, depths = ancestry_of(parents)
    positions = (seq_length + accepted).astype(jnp.float32)[:, None] + depths
    rotated_q = rotate(queries.astype(jnp.float32), positions)
    rotated_k = rotate(key_rows.astype(jnp.float32), positions) * head_dim ** (-0.5)
    scores = jnp.einsum("bihd,bjhd->bhij", rotated_q, rotated_k, precision=HIGH)
    spacing = jnp.maximum(depths[:, :, None] - depths[:, None, :], 0.0)
    weighting = ancestry[:, None] * jnp.exp(-decays[None, :, None, None] * spacing[:, None])
    within = jnp.einsum(
        "bhij,bjhe->bihe", scores * weighting, val_rows.astype(jnp.float32), precision=HIGH
    )
    state_scale = jnp.exp(-decays[None, None, :] * (depths[:, :, None] + 1.0))
    from_state = (
        jnp.einsum("bihd,bhde->bihe", rotated_q, carried, precision=HIGH) * state_scale[..., None]
    )
    mixed_raw = within + from_state
    average = jnp.mean(mixed_raw, axis=-1, keepdims=True)
    centred = mixed_raw - average
    variance = jnp.mean(centred * centred, axis=-1, keepdims=True)
    normed = (centred * lax.rsqrt(variance + EPS)).reshape(nseq * props, heads * head_dim)
    gates = gate_rows.astype(jnp.float32).reshape(nseq * props, heads * head_dim)
    return (normed * jax.nn.silu(gates)).astype(jnp.bfloat16)


def per_device(
    tokens,
    norm_gain,
    w_query,
    w_key,
    w_value,
    w_gate,
    w_output,
    decay_rate,
    state,
    prev_keys,
    prev_values,
    accepted,
    parents,
    seq_length,
):
    weights = jnp.concatenate([w_query, w_key, w_value, w_gate], axis=1)
    columns = weights.shape[1]
    whole = lax.all_gather(tokens, ("kv", "tp"), axis=1, tiled=True).astype(jnp.float32)
    scale = lax.rsqrt(jnp.mean(whole * whole, axis=1, keepdims=True) + EPS)
    full_normed = (whole * scale * norm_gain[None, :]).astype(jnp.bfloat16)
    projected = jnp.dot(full_normed, weights, preferred_element_type=jnp.float32)
    rows_count = tokens.shape[0]
    projected = projected.astype(jnp.bfloat16).reshape(rows_count, 4, columns // 4)
    regrouped = lax.all_to_all(projected, ("kv", "tp"), split_axis=0, concat_axis=2, tiled=True)
    nseq = state.shape[0]
    heads = decay_rate.shape[0]
    head_dim = state.shape[2]
    props = parents.shape[1]

    def shaped(role):
        return regrouped[:, role].reshape(nseq, props, heads, head_dim)

    carried = advance(state, prev_keys, prev_values, accepted, decay_rate)
    mixed = retain(
        shaped(0),
        shaped(1),
        shaped(2),
        shaped(3),
        decay_rate,
        carried,
        parents,
        accepted,
        seq_length,
    )
    output = jnp.dot(
        lax.all_gather(mixed, ("kv", "tp"), axis=0, tiled=True),
        w_output,
        preferred_element_type=jnp.float32,
    ).astype(jnp.bfloat16)
    return (output, carried)


def solution(mesh):
    placed = (
        P("dp", ("kv", "tp")),
        P(),
        P(None, ("kv", "tp")),
        P(None, ("kv", "tp")),
        P(None, ("kv", "tp")),
        P(None, ("kv", "tp")),
        P(None, ("kv", "tp")),
        P(),
        P(("dp", "kv", "tp"), None, None, None),
        P(("dp", "kv", "tp"), None, None),
        P(("dp", "kv", "tp"), None, None),
        P(("dp", "kv", "tp")),
        P(("dp", "kv", "tp"), None),
        P(("dp", "kv", "tp")),
    )
    return jax.shard_map(
        per_device,
        mesh=mesh,
        in_specs=placed,
        out_specs=(P("dp", ("kv", "tp")), P(("dp", "kv", "tp"), None, None, None)),
        check_vma=False,
    )
```

profile of v0, /device:TPU:0, one launch (start us, length us, event | category | flops | bytes accessed | tf_op | source)
XLA Modules:
  0.0 55.8 jit_solution(4770530740804355256)
XLA Ops:
  0.6 0.0 copy-start
  0.6 16.3 %all_gather.6 = bf16[32,4096]{1,0:T(8,128)(2,1)S(1)} all-gather(bf16[32,512]{1,0:T(8,128)(2,1)} %param.14), channel_id=1, replica_groups=mesh['dp'=4,'kv'=4,'tp'=2] {'kv','tp'}, dimensions={1}, use_global_device_ids=true | all-gather | bytes 294912 | tf_op jit(solution)/shard_map/all_gather | solution.py:98
  16.9 0.2 fusion.20
  17.1 6.3 %fusion.8 = bf16[32,1536]{1,0:T(8,128)(2,1)S(1)} fusion(bf16[4096,384]{1,0:T(8,128)(2,1)} %param.19, bf16[4096,384]{1,0:T(8,128)(2,1)} %param.18, bf16[4096,384]{1,0:T(8,128)(2,1)} %param.17, bf16[4096,384]{1,0:T(8,128)(2,1)} %param.16, bf16[32,4096]{1,0:T(8,128)(2,1)S(1)} %all_gather.6, f32[4096]{0:T(1024)} %param.15, f32[32]{0:T(128)S(1)} %add_rsqrt_fusion.1), kind=kOutput, calls=%fused_computation.8 | convolution fusion | flops 453558272 | bytes 12959872 | tf_op jit(solution)/shard_map/dot_general | solution.py:101
  23.5 0.7 %reshape.477 = bf16[32,4,384]{2,1,0:T(4,128)(2,1)} reshape(bf16[32,1536]{1,0:T(8,128)(2,1)S(1)} %fusion.8) | data formatting | bytes 196608 | tf_op jit(solution)/shard_map/reshape | solution.py:103
  24.1 4.7 %all-to-all-start = ((bf16[32,4,384]{2,1,0:T(4,128)(2,1)}), bf16[32,4,384]{2,1,0:T(4,128)(2,1)S(1)}, u32[]{:S(2)}, u32[]{:S(2)}) async-start(bf16[32,4,384]{2,1,0:T(4,128)(2,1)} %reshape.477), calls=%async_computation | async-start | bytes 196608 | tf_op jit(solution)/shard_map/all_to_all | solution.py:104
  30.2 0.3 fusion.39
  30.4 0.3 fusion.38
  30.7 0.3 fusion.50
  31.0 0.1 copy.41
  31.1 0.1 multiply_cosine_fusion
  31.2 0.1 multiply_exponential_fusion
  31.3 4.2 %bitcast_add_fusion = f32[1,24,128,128]{3,2,1,0:T(8,128)} fusion(f32[1,24,128,128]{3,2,1,0:T(8,128)} %param.22, f32[24]{0:T(128)S(1)} %get-tuple-element.23, bf16[1,4,3072]{2,1,0:T(4,128)(2,1)S(1)} %copy-done.1, bf16[1,4,3072]{2,1,0:T(4,128)(2,1)S(1)} %copy-done.2, f32[4,24]{0,1:T(8,128)S(1)} %get-tuple-element.21), kind=kOutput, calls=%fused_computation.11 | convolution fusion | flops 19685376 | bytes 3195360 | tf_op jit(solution)/shard_map/bphd,bphe->bhde/dot_general | solution.py:51
  35.5 0.1 subtract_maximum_fusion
  35.6 0.2 slice_reduce_fusion
  35.8 0.1 fusion.47
  35.9 0.1 subtract_bitcast_fusion
  36.0 2.9 %fusion.17 = f32[1,4,24,128]{3,1,2,0:T(4,128)S(1)} fusion(f32[1,24,128,128]{3,2,1,0:T(8,128)} %bitcast_add_fusion, f32[4,24]{0,1:T(8,128)S(1)} %get-tuple-element.20, f32[1,4,24,64]{3,1,2,0:T(4,128)S(1)} %get-tuple-element.14, f32[1,4,24,64]{3,1,2,0:T(4,128)S(1)} %get-tuple-element.15), kind=kOutput, calls=%fused_computation.17 | convolution fusion | flops 18898944 | bytes 1671552 | tf_op jit(solution)/shard_map/bihd,bhde->bihe/dot_general | solution.py:69
  38.8 0.4 convolution_multiply_fusion
  39.2 0.3 fusion.51
  39.5 0.2 multiply_reduce_fusion
  39.7 0.1 fusion.37
  39.8 14.6 %all-gather = bf16[8,4,3072]{2,1,0:T(4,128)(2,1)S(1)} all-gather(bf16[1,4,3072]{2,1,0:T(4,128)(2,1)S(1)} %fusion.37), channel_id=1, replica_groups=mesh['dp'=4,'kv'=4,'tp'=2] {'kv','tp'}, dimensions={0}, use_global_device_ids=true | all-gather | bytes 221184 | tf_op jit(solution)/shard_map/all_gather | solution.py:126
  54.5 1.3 %convolution_convert_fusion = bf16[32,512]{1,0:T(8,128)(2,1)} fusion(bf16[32,3072]{1,0:T(8,128)(2,1)S(1)} %reshape.491, bf16[3072,512]{1,0:T(8,128)(2,1)S(1)} %copy-done), kind=kOutput, calls=%fused_computation.13 | convolution fusion | flops 100679680 | bytes 3375104 | tf_op jit(solution)/shard_map/dot_general | solution.py:125
  (20 shorter events, 0.2 us)
Async XLA Ops:
  0.6 53.9 %copy-start = (bf16[3072,512]{1,0:T(8,128)(2,1)S(1)}, bf16[3072,512]{1,0:T(8,128)(2,1)}, u32[]{:S(2)}) copy-start(bf16[3072,512]{1,0:T(8,128)(2,1)} %param.20) | copy-start | bytes 9437188
  17.1 13.1 %copy-start.3 = (f32[24]{0:T(128)S(1)}, f32[24]{0:T(128)}, u32[]{:S(2)}) copy-start(f32[24]{0:T(128)} %param.21) | copy-start | bytes 292
  17.1 13.1 %copy-start.4 = (s32[1,4]{1,0:T(1,128)S(1)}, s32[1,4]{1,0:T(1,128)}, u32[]{:S(2)}) copy-start(s32[1,4]{1,0:T(1,128)} %param.26) | copy-start | bytes 52
  17.1 14.2 %copy-start.1 = (bf16[1,4,3072]{2,1,0:T(4,128)(2,1)S(1)}, bf16[1,4,3072]{2,1,0:T(4,128)(2,1)}, u32[]{:S(2)}) copy-start(bf16[1,4,3072]{2,1,0:T(4,128)(2,1)} %param.23) | copy-start | bytes 73732
  17.1 14.2 %copy-start.2 = (bf16[1,4,3072]{2,1,0:T(4,128)(2,1)S(1)}, bf16[1,4,3072]{2,1,0:T(4,128)(2,1)}, u32[]{:S(2)}) copy-start(bf16[1,4,3072]{2,1,0:T(4,128)(2,1)} %param.24) | copy-start | bytes 73732
  24.1 11.4 %all-to-all-start = ((bf16[32,4,384]{2,1,0:T(4,128)(2,1)}), bf16[32,4,384]{2,1,0:T(4,128)(2,1)S(1)}, u32[]{:S(2)}, u32[]{:S(2)}) async-start(bf16[32,4,384]{2,1,0:T(4,128)(2,1)} %reshape.477), calls=%async_computation | async-start | bytes 196608 | tf_op jit(solution)/shard_map/all_to_all | solution.py:104
where the time goes:
time: 56.1 us; the launch traced here: 55.8 us
  blocking collectives  30.9 us (55%)
  matrix products  16.1 us (29%)
  starting transfers between devices  4.68 us (8%)
  between operations  2.12 us (4%)
  other arithmetic  1.07 us (2%)
  local copies, waits for them, and re-layouts  0.95 us (2%)
    all_gather x1, blocking collectives, per_device(): lax.all_gather(tokens, ('kv', 'tp'), axis=1, tiled=True).astype(jnp.float32)  16.3 us
    all_gather x1, blocking collectives, per_device(): lax.all_gather(mixed, ('kv', 'tp'), axis=0, tiled=True)  14.6 us
    dot_general x1, matrix products, per_device(): jnp.dot(full_normed, weights, preferred_element_type=jnp.float32)  6.34 us
    all_to_all x1, starting transfers between devices, per_device(): lax.all_to_all(projected, ('kv', 'tp'), split_axis=0, concat_axis=2, tile...  4.68 us
    dot_general x1, matrix products, advance(): jnp.einsum('bphd,bphe->bhde', old_keys * weights[..., None], old_values,...  4.16 us
    dot_general x1, matrix products, retain(): jnp.einsum('bihd,bhde->bihe', rotated_q, carried, precision=HIGH)  2.85 us
    dot_general x1, matrix products, per_device(): jnp.dot(lax.all_gather(mixed, ('kv', 'tp'), axis=0, tiled=True), w_output...  1.26 us
  transfers between devices with their start and end apart: 1, of which 0 were waited for; matrix products, arithmetic and copies ran while one was open for 10% of the time, Pallas kernels for 0%

commit v1 on v0

--- a/solution.py
+++ b/solution.py
@@ -101,7 +101,9 @@
     projected = jnp.dot(full_normed, weights, preferred_element_type=jnp.float32)
     rows_count = tokens.shape[0]
     projected = projected.astype(jnp.bfloat16).reshape(rows_count, 4, columns // 4)
-    regrouped = lax.all_to_all(projected, ("kv", "tp"), split_axis=0, concat_axis=2, tiled=True)
+    shards = jnp.split(projected, lax.axis_size(("kv", "tp")), axis=0)
+    received = lax.all_to_all(jnp.stack(shards), ("kv", "tp"), 0, 0)
+    regrouped = jnp.concatenate(received, axis=2)
     nseq = state.shape[0]
     heads = decay_rate.shape[0]
     head_dim = state.shape[2]

time: 56.1 us -> 60.5 us (1.078)
  local copies, waits for them, and re-layouts: 0.95 us -> 5.27 us
    unnamed x11 -> x18, local copies, waits for them, and re-layouts: 0.08 us -> 4.31 us
    another operation x0 -> x9, local copies, waits for them, and re-layouts: none -> 0.71 us  [per_device(): received = lax.all_to_all(jnp.stack(shards), ('kv', 'tp'), 0, 0)]
    reshape x1, local copies, waits for them, and re-layouts: 0.65 us -> 0.04 us  [per_device(): regrouped = jnp.concatenate(received, axis=2)]
  transfers between devices with their start and end apart: 1 -> 1, of which waited for: 0 -> 0; matrix products, arithmetic and copies ran while one was open for 10% -> 9% of each run, Pallas kernels for 0% -> 0%
where the time goes in v1:
time: 60.5 us; the launch traced here: 60.2 us
  blocking collectives  30.9 us (51%)
  matrix products  16.1 us (27%)
  local copies, waits for them, and re-layouts  5.27 us (9%)
  starting transfers between devices  4.68 us (8%)
  between operations  2.16 us (4%)
  other arithmetic  1.07 us (2%)
    all_gather x1, blocking collectives, per_device(): lax.all_gather(tokens, ('kv', 'tp'), axis=1, tiled=True).astype(jnp.float32)  16.3 us
    all_gather x1, blocking collectives, per_device(): lax.all_gather(mixed, ('kv', 'tp'), axis=0, tiled=True)  14.6 us
    dot_general x1, matrix products, per_device(): jnp.dot(full_normed, weights, preferred_element_type=jnp.float32)  6.34 us
    all_to_all x1, starting transfers between devices, per_device(): received = lax.all_to_all(jnp.stack(shards), ('kv', 'tp'), 0, 0)  4.68 us
    unnamed x18, local copies, waits for them, and re-layouts  4.31 us
    dot_general x1, matrix products, advance(): jnp.einsum('bphd,bphe->bhde', old_keys * weights[..., None], old_values,...  4.16 us
    dot_general x1, matrix products, retain(): jnp.einsum('bihd,bhde->bihe', rotated_q, carried, precision=HIGH)  2.85 us
    dot_general x1, matrix products, per_device(): jnp.dot(lax.all_gather(mixed, ('kv', 'tp'), axis=0, tiled=True), w_output...  1.26 us
  transfers between devices with their start and end apart: 1, of which 0 were waited for; matrix products, arithmetic and copies ran while one was open for 9% of the time, Pallas kernels for 0%

profile of v1, /device:TPU:0, one launch (start us, length us, event | category | flops | bytes accessed | tf_op | source)
XLA Modules:
  0.0 60.2 jit_solution(9756254841239469667)
XLA Ops:
  0.6 16.3 %all_gather.6 = bf16[32,4096]{1,0:T(8,128)(2,1)S(1)} all-gather(bf16[32,512]{1,0:T(8,128)(2,1)} %param.14), channel_id=1, replica_groups=mesh['dp'=4,'kv'=4,'tp'=2] {'kv','tp'}, dimensions={1}, use_global_device_ids=true | all-gather | bytes 294912 | tf_op jit(solution)/shard_map/all_gather | solution.py:98
  16.9 0.2 fusion.20
  17.1 6.3 %fusion.8 = bf16[32,1536]{1,0:T(8,128)(2,1)S(1)} fusion(bf16[4096,384]{1,0:T(8,128)(2,1)} %param.19, bf16[4096,384]{1,0:T(8,128)(2,1)} %param.18, bf16[4096,384]{1,0:T(8,128)(2,1)} %param.17, bf16[4096,384]{1,0:T(8,128)(2,1)} %param.16, bf16[32,4096]{1,0:T(8,128)(2,1)S(1)} %all_gather.6, f32[4096]{0:T(1024)} %param.15, f32[32]{0:T(128)S(1)} %add_rsqrt_fusion.1), kind=kOutput, calls=%fused_computation.8 | convolution fusion | flops 453558272 | bytes 12959872 | tf_op jit(solution)/shard_map/dot_general | solution.py:101
  23.7 0.6 %constant_dynamic-update-slice_fusion.7 = bf16[8,4,4,384]{3,2,1,0:T(4,128)(2,1)} fusion(bf16[1,4,4,384]{3,2,1,0:T(4,128)(2,1)S(1)} %stack.27), kind=kLoop, calls=%fused_computation.59 | loop fusion | bytes 24576
  24.3 0.6 %constant_dynamic-update-slice_fusion.6 = bf16[8,4,4,384]{3,2,1,0:T(4,128)(2,1)} fusion(bf16[8,4,4,384]{3,2,1,0:T(4,128)(2,1)} %constant_dynamic-update-slice_fusion.7, bf16[1,4,4,384]{3,2,1,0:T(4,128)(2,1)S(1)} %stack.28), kind=kLoop, calls=%fused_computation.58 | loop fusion | bytes 24576
  24.9 0.6 constant_dynamic-update-slice_fusion.5
  25.5 0.6 constant_dynamic-update-slice_fusion.4
  26.1 0.6 %constant_dynamic-update-slice_fusion.3 = bf16[8,4,4,384]{3,2,1,0:T(4,128)(2,1)} fusion(bf16[8,4,4,384]{3,2,1,0:T(4,128)(2,1)} %constant_dynamic-update-slice_fusion.4, bf16[1,4,4,384]{3,2,1,0:T(4,128)(2,1)S(1)} %stack.31), kind=kLoop, calls=%fused_computation.55 | loop fusion | bytes 24576
  26.7 0.6 %constant_dynamic-update-slice_fusion.2 = bf16[8,4,4,384]{3,2,1,0:T(4,128)(2,1)} fusion(bf16[8,4,4,384]{3,2,1,0:T(4,128)(2,1)} %constant_dynamic-update-slice_fusion.3, bf16[1,4,4,384]{3,2,1,0:T(4,128)(2,1)S(1)} %stack.32), kind=kLoop, calls=%fused_computation.54 | loop fusion | bytes 24576
  27.3 0.6 %constant_dynamic-update-slice_fusion.1 = bf16[8,4,4,384]{3,2,1,0:T(4,128)(2,1)} fusion(bf16[8,4,4,384]{3,2,1,0:T(4,128)(2,1)} %constant_dynamic-update-slice_fusion.2, bf16[1,4,4,384]{3,2,1,0:T(4,128)(2,1)S(1)} %stack.33), kind=kLoop, calls=%fused_computation.53 | loop fusion | bytes 24576
  27.9 0.6 constant_dynamic-update-slice_fusion
  28.5 4.7 %all-to-all-start = ((bf16[8,4,4,384]{3,2,1,0:T(4,128)(2,1)}), bf16[8,4,4,384]{3,2,1,0:T(4,128)(2,1)S(1)}, u32[]{:S(2)}, u32[]{:S(2)}) async-start(bf16[8,4,4,384]{3,2,1,0:T(4,128)(2,1)} %constant_dynamic-update-slice_fusion), calls=%async_computation | async-start | bytes 196608 | tf_op jit(solution)/shard_map/all_to_all | solution.py:105
  34.6 0.3 fusion.39
  34.8 0.3 fusion.38
  35.1 0.3 fusion.51
  35.7 4.2 %bitcast_add_fusion = f32[1,24,128,128]{3,2,1,0:T(8,128)} fusion(f32[1,24,128,128]{3,2,1,0:T(8,128)} %param.22, f32[24]{0:T(128)S(1)} %get-tuple-element.31, bf16[1,4,3072]{2,1,0:T(4,128)(2,1)S(1)} %copy-done.1, bf16[1,4,3072]{2,1,0:T(4,128)(2,1)S(1)} %copy-done.2, f32[4,24]{0,1:T(8,128)S(1)} %get-tuple-element.29), kind=kOutput, calls=%fused_computation.11 | convolution fusion | flops 19685376 | bytes 3195360 | tf_op jit(solution)/shard_map/bphd,bphe->bhde/dot_general | solution.py:51
  39.9 0.2 slice_reduce_fusion
  40.3 2.9 %fusion.17 = f32[1,4,24,128]{3,1,2,0:T(4,128)S(1)} fusion(f32[1,24,128,128]{3,2,1,0:T(8,128)} %bitcast_add_fusion, f32[4,24]{0,1:T(8,128)S(1)} %get-tuple-element.28, f32[1,4,24,64]{3,1,2,0:T(4,128)S(1)} %get-tuple-element.22, f32[1,4,24,64]{3,1,2,0:T(4,128)S(1)} %get-tuple-element.23), kind=kOutput, calls=%fused_computation.17 | convolution fusion | flops 18898944 | bytes 1671552 | tf_op jit(solution)/shard_map/bihd,bhde->bihe/dot_general | solution.py:69
  43.2 0.4 convolution_multiply_fusion
  43.6 0.3 fusion.52
  43.9 0.2 multiply_reduce_fusion
  44.1 0.1 fusion.37
  44.2 14.6 %all-gather = bf16[8,4,3072]{2,1,0:T(4,128)(2,1)S(1)} all-gather(bf16[1,4,3072]{2,1,0:T(4,128)(2,1)S(1)} %fusion.37), channel_id=1, replica_groups=mesh['dp'=4,'kv'=4,'tp'=2] {'kv','tp'}, dimensions={0}, use_global_device_ids=true | all-gather | bytes 221184 | tf_op jit(solution)/shard_map/all_gather | solution.py:128
  58.9 1.3 %convolution_convert_fusion = bf16[32,512]{1,0:T(8,128)(2,1)} fusion(bf16[32,3072]{1,0:T(8,128)(2,1)S(1)} %reshape.512, bf16[3072,512]{1,0:T(8,128)(2,1)S(1)} %copy-done), kind=kOutput, calls=%fused_computation.13 | convolution fusion | flops 100679680 | bytes 3375104 | tf_op jit(solution)/shard_map/dot_general | solution.py:127
  (36 shorter events, 0.8 us)
Async XLA Ops:
  0.6 58.3 %copy-start = (bf16[3072,512]{1,0:T(8,128)(2,1)S(1)}, bf16[3072,512]{1,0:T(8,128)(2,1)}, u32[]{:S(2)}) copy-start(bf16[3072,512]{1,0:T(8,128)(2,1)} %param.20) | copy-start | bytes 9437188
  17.1 17.4 %copy-start.3 = (f32[24]{0:T(128)S(1)}, f32[24]{0:T(128)}, u32[]{:S(2)}) copy-start(f32[24]{0:T(128)} %param.21) | copy-start | bytes 292
  17.1 17.5 %copy-start.4 = (s32[1,4]{1,0:T(1,128)S(1)}, s32[1,4]{1,0:T(1,128)}, u32[]{:S(2)}) copy-start(s32[1,4]{1,0:T(1,128)} %param.26) | copy-start | bytes 52
  17.1 18.5 %copy-start.1 = (bf16[1,4,3072]{2,1,0:T(4,128)(2,1)S(1)}, bf16[1,4,3072]{2,1,0:T(4,128)(2,1)}, u32[]{:S(2)}) copy-start(bf16[1,4,3072]{2,1,0:T(4,128)(2,1)} %param.23) | copy-start | bytes 73732
  17.1 18.5 %copy-start.2 = (bf16[1,4,3072]{2,1,0:T(4,128)(2,1)S(1)}, bf16[1,4,3072]{2,1,0:T(4,128)(2,1)}, u32[]{:S(2)}) copy-start(bf16[1,4,3072]{2,1,0:T(4,128)(2,1)} %param.24) | copy-start | bytes 73732
  28.5 11.4 %all-to-all-start = ((bf16[8,4,4,384]{3,2,1,0:T(4,128)(2,1)}), bf16[8,4,4,384]{3,2,1,0:T(4,128)(2,1)S(1)}, u32[]{:S(2)}, u32[]{:S(2)}) async-start(bf16[8,4,4,384]{3,2,1,0:T(4,128)(2,1)} %constant_dynamic-update-slice_fusion), calls=%async_computation | async-start | bytes 196608 | tf_op jit(solution)/shard_map/all_to_all | solution.py:105
